TPU v7x, 32 devices: a whole 2x2x4 slice. The times are simulated.
32 devices in a mesh: grp: 2 (over y), sp: 4 (over z), tp: 4 (over x, core).
Axes of the slice: x: 2, y: 2, z: 4, core: 2. Of those that a mesh axis runs over, the one named last changes fastest.
Arguments:
- queries: bfloat16 [2048, 1024], P(('grp', 'sp'), 'tp'), parts along dimension 0, may hold values from -7 to 10
- keys: bfloat16 [2048, 1024], P(('grp', 'sp'), 'tp'), parts along dimension 0, may hold values from -14 to 7
- values: bfloat16 [2048, 1024], P(('grp', 'sp'), 'tp'), parts along dimension 0, may hold values from -6 to 6
- resid: bfloat16 [2048, 2048], P(('grp', 'sp', 'tp')), parts along dimension 0, may hold values from -18 to 18
- out_weight: bfloat16 [1024, 2048], P('tp'), may hold values from -0.375 to 0.375
- gate_weight: bfloat16 [2048, 3072], P('sp', 'tp'), may hold values from -0.125 to 0.125
- value_weight: bfloat16 [2048, 3072], P('sp', 'tp'), may hold values from -0.125 to 0.125
- conv_gate: float32 [3, 3072], P(None, 'tp'), may hold values from -3 to 3
- conv_value: float32 [3, 3072], P(None, 'tp'), may hold values from -3 to 3
- norm_gain: float32 [2048], replicated, may hold values from 0.1 to 1.9
- down_weight: bfloat16 [3072, 2048], P('tp', 'sp'), may hold values from -0.109375 to 0.109375
Outputs:
- layer_out: bfloat16 [2048, 2048], P(('grp', 'sp', 'tp')), parts along dimension 0
There are 2 independent parts, one for each index of `grp`. A program takes and returns all parts, laid end to end along the dimension named above; an argument that names none is the same for every part. Nothing has to cross between parts.
All inputs are finite; a program needn't handle non-finite values.
Results may differ from a plain program's by a relative error of at most 0.0058.
Values may be sent and summed in bfloat16 or wider, within the bound.
A program may use at most 128 MiB of HBM per device.

v0:
```python
import jax
import jax.numpy as jnp
from jax import lax
from jax.sharding import PartitionSpec as P

HEAD = 64


epsilon = 1e-06


def shifted(block, axis, distance):
    devices = range(lax.axis_size(axis))
    route = [(i - distance, i) for i in devices if i - distance in devices]
    return lax.ppermute(block, axis, route)


def block_terms(query_rows, key_rows, value_rows, query_place, key_place):
    scores = jnp.einsum(
        "qhe,khe->hqk", query_rows, key_rows, preferred_element_type=jnp.float32
    ) * HEAD ** (-0.5)
    causal = (key_place[None, :] < query_place[:, None])[None]
    stay_log = jnp.where(causal, jax.nn.log_sigmoid(-scores), 0.0)
    suffix = lax.cumsum(stay_log, axis=2, reverse=True) - stay_log
    local_weight = jnp.where(causal, jnp.exp(jax.nn.log_sigmoid(scores) + suffix), 0.0).astype(
        jnp.bfloat16
    )
    part = jnp.einsum("hqk,khe->hqe", local_weight, value_rows, preferred_element_type=jnp.float32)
    return (jnp.sum(stay_log, axis=2), part)


def normalize(state, norm_gain):
    values = state.astype(jnp.float32)
    scaled = values * lax.rsqrt(jnp.mean(values * values, axis=-1, keepdims=True) + epsilon)
    return (scaled * norm_gain).astype(jnp.bfloat16)


def causal_conv(rim_rows, rows, taps):
    extended = jnp.concatenate([rim_rows, rows], axis=0).astype(jnp.float32)
    length = rows.shape[0]
    total = jnp.zeros(rows.shape, jnp.float32)
    for start_displacement in range(taps.shape[0]):
        total = (
            total
            + taps[start_displacement] * extended[start_displacement : start_displacement + length]
        )
    return total


def body(
    queries,
    keys,
    values,
    resid,
    out_weight,
    gate_weight,
    value_weight,
    conv_gate,
    conv_value,
    norm_gain,
    down_weight,
):
    tok_dev = queries.shape[0]
    mix_local = queries.shape[1]
    head_count = mix_local // HEAD
    sp_count = lax.axis_size("sp")
    block = tok_dev * min(sp_count, max(1, 1024 // tok_dev))
    paired = jnp.concatenate([keys, values], axis=1)
    gathered = lax.all_gather(paired, "sp", axis=0, tiled=True)
    mine = lax.axis_index("sp")
    query_place = mine * tok_dev + jnp.arange(tok_dev, dtype=jnp.int32)
    query_rows = queries.reshape(tok_dev, head_count, HEAD)

    def add_block(index, carry):
        start = index * block
        piece = lax.dynamic_slice_in_dim(gathered, start, block, 0)
        key_rows = piece[:, :mix_local].reshape(block, head_count, HEAD)
        value_rows = piece[:, mix_local:].reshape(block, head_count, HEAD)
        key_place = start + jnp.arange(block, dtype=jnp.int32)
        total, part = block_terms(query_rows, key_rows, value_rows, query_place, key_place)
        return carry * jnp.exp(total)[:, :, None] + part

    start_carry = jnp.zeros((head_count, tok_dev, HEAD), jnp.float32)
    attended = lax.fori_loop(0, mine * tok_dev // block + 1, add_block, start_carry)
    mixed = jnp.transpose(attended, (1, 0, 2)).reshape(tok_dev, mix_local).astype(jnp.bfloat16)
    projected = lax.psum_scatter(
        jnp.dot(mixed, out_weight, preferred_element_type=jnp.float32),
        "tp",
        scatter_dimension=0,
        tiled=True,
    )
    state = (resid.astype(jnp.float32) + projected).astype(jnp.bfloat16)
    normed = lax.all_gather(normalize(state, norm_gain), "tp", axis=0, tiled=True)
    ff_local = gate_weight.shape[1]
    gate_full = jnp.dot(
        normed,
        lax.all_gather(gate_weight, "sp", axis=0, tiled=True),
        preferred_element_type=jnp.float32,
    )
    value_full = jnp.dot(
        normed,
        lax.all_gather(value_weight, "sp", axis=0, tiled=True),
        preferred_element_type=jnp.float32,
    )
    gate_pre = gate_full.astype(jnp.bfloat16)
    value_pre = value_full.astype(jnp.bfloat16)
    taps_count = conv_gate.shape[0]
    rim = jnp.concatenate(
        [gate_pre[tok_dev - taps_count + 1 :], value_pre[tok_dev - taps_count + 1 :]], axis=1
    )
    before = shifted(rim, "sp", 1)
    conv_gate_out = causal_conv(before[:, :ff_local], gate_pre, conv_gate)
    conv_value_out = causal_conv(before[:, ff_local:], value_pre, conv_value)
    gated = (jax.nn.silu(conv_gate_out) * conv_value_out).astype(jnp.bfloat16)
    partial_sum = jnp.dot(
        gated,
        lax.all_gather(down_weight, "sp", axis=1, tiled=True),
        preferred_element_type=jnp.float32,
    )
    ffn_share = lax.psum_scatter(partial_sum, "tp", scatter_dimension=0, tiled=True)
    return (state.astype(jnp.float32) + ffn_share).astype(jnp.bfloat16)


def solution(mesh):
    placed = (
        P(("grp", "sp"), "tp"),
        P(("grp", "sp"), "tp"),
        P(("grp", "sp"), "tp"),
        P(("grp", "sp", "tp"), None),
        P("tp", None),
        P("sp", "tp"),
        P("sp", "tp"),
        P(None, "tp"),
        P(None, "tp"),
        P(),
        P("tp", "sp"),
    )
    return jax.shard_map(
        body, mesh=mesh, in_specs=placed, out_specs=P(("grp", "sp", "tp"), None), check_vma=False
    )
```

profile of v0, /device:TPU:0, one launch (start us, length us, event | category | flops | bytes accessed | tf_op | source)
XLA Modules:
  0.0 383.4 jit_solution(949477178948924257)
XLA Ops:
  6.5 1.1 copy.14
  7.6 1.0 copy.15
  8.6 0.7 pad_maximum_fusion
  9.5 1.0 copy.16
  10.5 31.7 %all-gather.6.cloned.1.call-done = bf16[1024,512]{0,1:T(8,128)(2,1)} async-done(((bf16[256,512]{0,1:T(8,128)(2,1)}), bf16[1024,512]{0,1:T(8,128)(2,1)}) %all-gather.6.cloned.1.call-update) | async-done | bytes 1048592 | tf_op jit(solution)/shard_map/all_gather | solution.py:69
  42.2 56.0 %while.11 = (s32[]{:T(128)}, f32[4,256,64]{1,2,0:T(8,128)S(1)}, s32[]{:T(128)}, bf16[1024,512]{0,1:T(8,128)(2,1)}, bf16[256,4,64]{0,2,1:T(8,128)(2,1)S(1)}, /*index=5*/s32[]{:T(128)}, s32[]{:T(128)}, s32[]{:T(128)}, f32[]{:T(128)}) while((s32[]{:T(128)}, f32[4,256,64]{1,2,0:T(8,128)S(1)}, s32[]{:T(128)}, ...), condition=%wide.region_4.5_spmd.clone, body=%wide.region_0.4_spmd.clone.sunk | while | flops 447937792 | bytes 93714576 | solution.py:84
  42.2 1.3 fusion.66
  43.5 2.9 fusion.67
  46.6 5.6 %fusion.68 = (f32[4,256]{1,0:T(4,128)S(1)}, f32[4,256,1024]{2,1,0:T(8,128)S(1)}) fusion(f32[4,256,1024]{2,1,0:T(8,128)} %get-tuple-element.134, u8[256,1024]{1,0:T(8,128)(4,1)S(1)} %get-tuple-element.135, pred[256,1024]{1,0:T(8,128)(4,1)S(1)} %broadcast_compare_fusion.2), kind=kLoop, calls=%fused_computation.20.clone.1 | loop fusion | flops 13630464 | bytes 8916992 | tf_op jit(solution)/shard_map/while/body/reduce_sum | solution.py:29
  52.3 3.0 copy.21
  55.2 5.5 %copy.22 = f32[4,256,8,128]{1,2,3,0:T(8,128)} copy(f32[4,256,8,128]{3,2,1,0:T(8,128)} %bitcast.44) | data formatting | bytes 8388608 | tf_op jit(solution)/shard_map/reshape
  60.8 10.8 %fusion.69 = f32[4,256,8,128]{1,2,3,0:T(8,128)S(1)} fusion(f32[4,256,8,128]{1,2,3,0:T(8,128)} %copy.22), kind=kOutput, calls=%fused_computation.65.clone.1 | output fusion | flops 133169152 | bytes 8388608 | tf_op jit(solution)/shard_map/reduce-window
  71.6 2.0 copy-done.1
  73.6 4.5 %broadcast_add_fusion.2 = f32[4,256,8,128]{1,2,3,0:T(8,128)} fusion(f32[4,256,8,128]{1,2,3,0:T(8,128)} %copy-done.1, f32[4,256,8]{1,2,0:T(8,128)S(1)} %slice.148), kind=kLoop, calls=%fused_computation.10.clone.1 | loop fusion | flops 1048576 | bytes 8421376 | tf_op jit(solution)/shard_map/reduce_window_sum | solution.py:24
  78.1 5.5 %copy.23 = f32[4,256,8,128]{3,2,1,0:T(8,128)} copy(f32[4,256,8,128]{1,2,3,0:T(8,128)} %broadcast_add_fusion.2) | data formatting | bytes 8388608 | tf_op jit(solution)/shard_map/reduce_window_sum | solution.py:24
  83.6 4.9 %reduce_window_sum.20 = f32[4,256,1024]{2,1,0:T(8,128)} reshape(f32[4,256,8,128]{3,2,1,0:T(8,128)} %copy.23) | data formatting | bytes 8388608 | tf_op jit(solution)/shard_map/reduce_window_sum | solution.py:24
  88.5 9.5 %fusion.70 = f32[4,256,64]{1,2,0:T(8,128)S(1)} fusion(bf16[1024,4,64]{0,2,1:T(8,128)(2,1)S(1)} %bitcast.46, f32[4,256,1024]{2,1,0:T(8,128)} %reduce_window_sum.20, f32[4,256,1024]{2,1,0:T(8,128)} %get-tuple-element.134, pred[256,1024]{1,0:T(8,128)(4,1)S(1)} %broadcast_compare_fusion.2, f32[4,256,64]{1,2,0:T(8,128)S(1)} %get-tuple-element.148, ...), kind=kOutput, calls=%fused_computation.12.clone.1 | convolution fusion | flops 159514624 | bytes 9965568 | tf_op jit(solution)/shard_map/while/body/hqk,khe->hqe/dot_general | solution.py:28
  98.3 1.8 fusion.39
  100.9 28.8 %reduce-scatter.3.cloned.1.call-done = f32[64,2048]{1,0:T(8,128)} async-done(((f32[256,2048]{1,0:T(8,128)}), f32[64,2048]{1,0:T(8,128)}) %reduce-scatter.3.cloned.1.call-update) | async-done | bytes 524304 | tf_op jit(solution)/shard_map/reduce_scatter | solution.py:86
  129.8 1.2 fusion.22
  131.0 0.8 fusion.24
  133.1 61.7 %all-gather.10.cloned.1.call-done = bf16[2048,768]{1,0:T(8,128)(2,1)} async-done(((bf16[512,768]{1,0:T(8,128)(2,1)}), bf16[2048,768]{1,0:T(8,128)(2,1)}) %all-gather.10.cloned.1.call-update) | async-done | bytes 3145744 | tf_op jit(solution)/shard_map/all_gather | solution.py:97
  194.8 16.8 %all-gather.8.cloned.1.call-done = bf16[256,2048]{1,0:T(8,128)(2,1)} async-done(((bf16[64,2048]{1,0:T(8,128)(2,1)}), bf16[256,2048]{1,0:T(8,128)(2,1)}) %all-gather.8.cloned.1.call-update) | async-done | bytes 1048592 | tf_op jit(solution)/shard_map/all_gather | solution.py:93
  211.6 3.3 convolution_convert_fusion.1
  215.0 61.6 %all-gather.12.cloned.1.call-done = bf16[2048,768]{1,0:T(8,128)(2,1)} async-done(((bf16[512,768]{1,0:T(8,128)(2,1)}), bf16[2048,768]{1,0:T(8,128)(2,1)}) %all-gather.12.cloned.1.call-update) | async-done | bytes 3145744 | tf_op jit(solution)/shard_map/all_gather | solution.py:102
  276.5 2.9 convolution_convert_fusion
  279.4 1.3 collective-permute-start
  280.8 1.2 collective-permute-done
  282.2 57.8 %all-gather.14.cloned.1.call-done = bf16[768,2048]{1,0:T(8,128)(2,1)} async-done(((bf16[768,512]{1,0:T(8,128)(2,1)}), bf16[768,2048]{1,0:T(8,128)(2,1)}) %all-gather.14.cloned.1.call-update) | async-done | bytes 3145744 | tf_op jit(solution)/shard_map/all_gather | solution.py:117
  340.1 4.7 %fusion.26 = f32[256,2048]{1,0:T(8,128)} fusion(bf16[768,2048]{1,0:T(8,128)(2,1)} %all-gather.14.cloned.1.call-done, f32[258,768]{1,0:T(8,128)S(1)} %get-tuple-element.84, f32[258,768]{1,0:T(8,128)S(1)} %get-tuple-element.83, f32[768]{0:T(1024)S(1)} %get-tuple-element.59, f32[768]{0:T(1024)S(1)} %get-tuple-element.60, f32[768]{0:T(1024)S(1)} %get-tuple-element.58, ...), kind=kOutput, calls=%fused_computation.45 | convolution fusion | flops 808452096 | bytes 9986048 | tf_op jit(solution)/shard_map/dot_general | solution.py:115
  344.8 30.0 %reduce-scatter.5.cloned.1.call-done = f32[64,2048]{1,0:T(8,128)} async-done(((f32[256,2048]{1,0:T(8,128)}), f32[64,2048]{1,0:T(8,128)}) %reduce-scatter.5.cloned.1.call-update) | async-done | bytes 524304 | tf_op jit(solution)/shard_map/reduce_scatter | solution.py:120
  374.8 1.8 fusion.25
  (43 shorter events, 2.7 us)
Async XLA Ops:
  6.5 91.8 %copy-start = (bf16[256,2048]{1,0:T(8,128)(2,1)S(1)}, bf16[256,2048]{1,0:T(8,128)(2,1)}, u32[]{:S(2)}) copy-start(bf16[256,2048]{1,0:T(8,128)(2,1)} %param.17) | copy-start | bytes 3145732
  6.5 35.7 %all-gather.6.cloned.1.call-start = ((), (), s32[]{:S(2)}) async-start(), calls=%async_computation.2 | async-start | bytes 1310720 | tf_op jit(solution)/shard_map/all_gather | solution.py:69
  9.4 120.4 %reduce-scatter.3.cloned.1.call-start = ((), (), s32[]{:S(2)}) async-start(), calls=%async_computation.3 | async-start | bytes 2621440 | tf_op jit(solution)/shard_map/reduce_scatter | solution.py:86
  71.6 2.0 copy-start.1
  98.2 31.5 %copy-start.2 = (bf16[64,2048]{1,0:T(8,128)(2,1)S(1)}, bf16[64,2048]{1,0:T(8,128)(2,1)}, u32[]{:S(2)}) copy-start(bf16[64,2048]{1,0:T(8,128)(2,1)} %param.16) | copy-start | bytes 786436
  98.3 32.8 %copy-start.3 = (f32[2048]{0:T(1024)S(1)}, f32[2048]{0:T(1024)}, u32[]{:S(2)}) copy-start(f32[2048]{0:T(1024)} %param.22) | copy-start | bytes 24580
  100.2 94.7 %all-gather.10.cloned.1.call-start = ((), (), s32[]{:S(2)}) async-start(), calls=%async_computation.5 | async-start | bytes 3932160 | tf_op jit(solution)/shard_map/all_gather | solution.py:97
  100.9 110.7 %all-gather.8.cloned.1.call-start = ((), (), s32[]{:S(2)}) async-start(), calls=%async_computation.4 | async-start | bytes 1310720 | tf_op jit(solution)/shard_map/all_gather | solution.py:93
  131.9 144.6 %all-gather.12.cloned.1.call-start = ((), (), s32[]{:S(2)}) async-start(), calls=%async_computation.6 | async-start | bytes 3932160 | tf_op jit(solution)/shard_map/all_gather | solution.py:102
  132.5 207.6 %all-gather.14.cloned.1.call-start = ((), (), s32[]{:S(2)}) async-start(), calls=%async_computation.7 | async-start | bytes 3932160 | tf_op jit(solution)/shard_map/all_gather | solution.py:117
  133.1 241.7 %reduce-scatter.5.cloned.1.call-start = ((), (), s32[]{:S(2)}) async-start(), calls=%async_computation.8 | async-start | bytes 2621440 | tf_op jit(solution)/shard_map/reduce_scatter | solution.py:120
  211.6 64.9 %copy-start.6 = (bf16[256,2048]{1,0:T(8,128)(2,1)S(1)}, bf16[256,2048]{1,0:T(8,128)(2,1)}, u32[]{:S(2)}) copy-start(bf16[256,2048]{1,0:T(8,128)(2,1)} %all-gather.8.cloned.1.call-done) | copy-start | bytes 3145732
  214.9 65.8 %copy-start.4 = (f32[3,768]{1,0:T(4,128)S(1)}, f32[3,768]{1,0:T(4,128)}, u32[]{:S(2)}) copy-start(f32[3,768]{1,0:T(4,128)} %param.21) | copy-start | bytes 27652
  214.9 65.8 %copy-start.5 = (f32[3,768]{1,0:T(4,128)S(1)}, f32[3,768]{1,0:T(4,128)}, u32[]{:S(2)}) copy-start(f32[3,768]{1,0:T(4,128)} %param.20) | copy-start | bytes 27652
  279.4 2.6 collective-permute-start
Sparse Core Ops, SparseCore 0:
  9.5 32.6 all-gather.5
  100.3 29.4 reduce-scatter.2
  131.4 63.4 all-gather.9
  196.3 15.3 all-gather.7
  213.0 63.4 all-gather.11
  278.0 62.0 all-gather.13
  344.9 29.8 reduce-scatter.4
where the time goes:
time: 384 us; the launch traced here: 383 us
  waiting for transfers between devices  292 us (76%)
  other arithmetic  25.9 us (7%)
  local copies, waits for them, and re-layouts  25.4 us (7%)
  matrix products  25.1 us (7%)
  between operations  13.7 us (4%)
    all_gather x1, waiting for transfers between devices, body(): lax.all_gather(gate_weight, 'sp', axis=0, tiled=True)  61.7 us
    all_gather x1, waiting for transfers between devices, body(): lax.all_gather(value_weight, 'sp', axis=0, tiled=True)  61.6 us
    all_gather x1, waiting for transfers between devices, body(): lax.all_gather(down_weight, 'sp', axis=1, tiled=True)  57.8 us
    all_gather x1, waiting for transfers between devices, body(): gathered = lax.all_gather(paired, 'sp', axis=0, tiled=True)  31.7 us
    reduce_scatter x1, waiting for transfers between devices, body(): lax.psum_scatter(partial_sum, 'tp', scatter_dimension=0, tiled=True)  30 us
    reduce_scatter x1, waiting for transfers between devices, body(): lax.psum_scatter(jnp.dot(mixed, out_weight, preferred_element_type=jnp.fl...  28.8 us
    all_gather x1, waiting for transfers between devices, body(): lax.all_gather(normalize(state, norm_gain), 'tp', axis=0, tiled=True)  16.8 us
    another operation x2, other arithmetic  10.9 us
  transfers between devices with their start and end apart: 8, of which 8 were waited for; matrix products, arithmetic and copies ran while one was open for 2% of the time, Pallas kernels for 0%

commit v1 on v0

--- a/solution.py
+++ b/solution.py
@@ -1,6 +1,10 @@
+import functools
+
 import jax
 import jax.numpy as jnp
 from jax import lax
+from jax.experimental import pallas as pl
+from jax.experimental.pallas import tpu as pltpu
 from jax.sharding import PartitionSpec as P
 
 HEAD = 64
@@ -121,6 +125,330 @@
     return (state.astype(jnp.float32) + ffn_share).astype(jnp.bfloat16)
 
 
+MESH = pl.DeviceIdType.MESH
+LANES = 128
+bf16, f32 = jnp.bfloat16, jnp.float32
+
+
+def mm(a, b):
+    return jnp.dot(a, b, preferred_element_type=f32)
+
+
+def layer_kernel(
+    n, qkv, up, down, ow, resid, gain, taps, out,
+    qkv_b, up_b, down_b, mix_s, mix_r, proj, op_s, op_r, nrm, pre, gated,
+    keep, c_s, c_r, x_s, x_r, z_s, z_r, state, send_sem, recv_sem,
+):
+    s, t, g = lax.axis_index("sp"), lax.axis_index("tp"), lax.axis_index("grp")
+    core = lax.rem(t, 2)
+    tc = t + 1 - 2 * core
+    tx = lax.rem(t + 2, 4)
+    tcx = lax.rem(tc + 2, 4)
+    tok = qkv.shape[1]
+    share = out.shape[0]
+    width = out.shape[1]
+    depth = up.shape[1]
+    half, dhalf = depth // 2, down.shape[1] // 2
+    ranks = list(range(1, n))
+    ahead = [lax.rem(s + d, n) for d in range(n)]
+    behind = [lax.rem(s + n - d, n) for d in range(n)]
+
+    barrier = pltpu.get_barrier_semaphore()
+    peers = [{"sp": ahead[d]} for d in ranks] + [{"tp": lax.rem(t + e, 4)} for e in (1, 2, 3)]
+    peers = peers + [{"grp": 1 - g}]
+    for peer in peers:
+        pl.semaphore_signal(barrier, inc=1, device_id=peer, device_id_type=MESH)
+    pl.semaphore_wait(barrier, len(peers))
+
+    names, started = {}, []
+
+    def slot(key):
+        return names.setdefault(key, len(names))
+
+    def remote(key, src, dst, peer):
+        i = slot(key)
+        return pltpu.make_async_remote_copy(
+            src_ref=src, dst_ref=dst, send_sem=send_sem.at[i], recv_sem=recv_sem.at[i],
+            device_id=peer, device_id_type=MESH,
+        )
+
+    def send(key, src, dst, peer):
+        copy = remote(key, src, dst, peer)
+        copy.start()
+        started.append(copy)
+
+    def receive(key, dst, peer):
+        remote(key, dst, dst, peer).wait_recv()
+
+    for d in ranks:
+        send(("q", d), qkv.at[ahead[d]], qkv_b.at[s], {"sp": ahead[d]})
+    for d in ranks:
+        rows = pl.ds(pl.multiple_of(half * g, half), half)
+        send(("u", d), up.at[ahead[d], rows], up_b.at[s, rows], {"sp": ahead[d]})
+    qkv_b[s] = qkv[s]
+    up_b[s] = up[s]
+    down_b[:, 2 * dhalf :] = jnp.zeros((n, down_b.shape[1] - 2 * dhalf, down_b.shape[2]), bf16)
+    down_b[s, : 2 * dhalf] = down[s]
+    pre[:8] = jnp.zeros((8, pre.shape[1]), f32)
+    for d in ranks:
+        receive(("q", d), qkv_b.at[behind[d]], {"sp": ahead[d]})
+
+    row = lax.broadcasted_iota(jnp.int32, (tok, tok), 0)
+    col = lax.broadcasted_iota(jnp.int32, (tok, tok), 1)
+    causal = col < row
+    later = jnp.where(row > col, 1.0, 0.0).astype(bf16)
+    lane = lax.broadcasted_iota(jnp.int32, (tok, LANES), 1)
+    even = lax.rem(s, 2) == 0
+    for i in range(n):
+        total = jnp.zeros((tok, LANES), f32)
+        carry = jnp.zeros((tok, 1), f32)
+        for j in range(i, -1, -1):
+            pair = qkv_b[j, :, LANES:]
+            score = lax.dot_general(
+                qkv_b[i, :, :LANES], pair, (((1,), (1,)), ((), ())), preferred_element_type=f32
+            ) * HEAD ** (-0.5)
+            soft = jnp.maximum(score, 0.0) + jnp.log(1.0 + jnp.exp(-jnp.abs(score)))
+            stay = jnp.where(causal, -soft, 0.0) if i == j else -soft
+            high = stay.astype(bf16)
+            low = (stay - high.astype(f32)).astype(bf16)
+            suffix = mm(high, later) + mm(low, later)
+            weight = jnp.exp(score - soft + suffix + carry)
+            if i == j:
+                weight = jnp.where(causal, weight, 0.0)
+            total = total + mm(weight.astype(bf16), pair)
+            if j > 0:
+                carry = carry + jnp.sum(stay, axis=1, keepdims=True)
+        low_half = jnp.where(lane < HEAD, pltpu.roll(total, HEAD, 1), 0.0)
+        high_half = jnp.where(lane < HEAD, 0.0, total)
+        mix_s[i] = jnp.where(even, low_half, high_half).astype(bf16)
+
+    for d in ranks:
+        send(("m", d), mix_s.at[ahead[d]], mix_r.at[s], {"sp": ahead[d]})
+    for d in ranks:
+        rows = pl.ds(pl.multiple_of(dhalf * g, dhalf), dhalf)
+        send(("d", d), down.at[ahead[d], rows], down_b.at[s, rows], {"sp": ahead[d]})
+    mix_r[s] = mix_s[s]
+    for d in ranks:
+        receive(("m", d), mix_r.at[behind[d]], {"sp": ahead[d]})
+
+    step = 512
+    pairs = [mix_r[2 * p] + mix_r[2 * p + 1] for p in range(n // 2)]
+    for k in range(width // step):
+        cols = slice(k * step, (k + 1) * step)
+        part = mm(pairs[0], ow[:LANES, cols])
+        for p in range(1, n // 2):
+            part = part + mm(pairs[p], ow[p * LANES : (p + 1) * LANES, cols])
+        proj[:, cols] = part
+
+    def chunk(at):
+        return pl.ds(pl.multiple_of(at * share, share), share)
+
+    for e in (2, 3, 1):
+        to = lax.rem(t + e, 4)
+        op_s[e - 1] = proj[chunk(to)].astype(bf16)
+        send(("o", e), op_s.at[e - 1], op_r.at[e - 1], {"tp": to})
+    across = {"grp": 1 - g}
+    for d in ranks:
+        rows = pl.ds(pl.multiple_of(half * g, half), half)
+        receive(("u", d), up_b.at[behind[d], rows], {"sp": ahead[d]})
+        send(("uy", d), up_b.at[behind[d], rows], up_b.at[behind[d], rows], across)
+    for e in (1, 2, 3):
+        receive(("o", e), op_r.at[e - 1], {"tp": lax.rem(t + e, 4)})
+    summed = proj[chunk(t)] + op_r[0].astype(f32) + op_r[1].astype(f32) + op_r[2].astype(f32)
+    state[...] = (resid[...].astype(f32) + summed).astype(bf16)
+    values = state[...].astype(f32)
+    scale = lax.rsqrt(jnp.mean(values * values, axis=-1, keepdims=True) + epsilon)
+
+    def block(si, ti):
+        return nrm.at[pl.ds(pl.multiple_of(si * tok + ti * share, share), share)]
+
+    nrm[pl.ds(pl.multiple_of(s * tok + t * share, share), share)] = (
+        values * scale * gain[...]
+    ).astype(bf16)
+    side, sib = {"tp": tx}, {"tp": tc}
+    order = [2, 1, 3] if n == 4 else ranks
+    for d in order:
+        send(("nz", d), block(s, t), block(s, t), {"sp": ahead[d]})
+    send(("nx", 0), block(s, t), block(s, t), side)
+    send(("nc", 0), block(s, t), block(s, t), sib)
+    for d in ranks:
+        rows = pl.ds(pl.multiple_of(dhalf * g, dhalf), dhalf)
+        receive(("d", d), down_b.at[behind[d], rows], {"sp": ahead[d]})
+        send(("dy", d), down_b.at[behind[d], rows], down_b.at[behind[d], rows], across)
+    receive(("nx", 0), block(s, tx), side)
+    send(("ncx", 0), block(s, tx), block(s, tx), sib)
+    for d in ranks:
+        rows = pl.ds(pl.multiple_of(half - half * g, half), half)
+        receive(("uy", d), up_b.at[behind[d], rows], across)
+
+    def lift(si):
+        at = pl.multiple_of(si * tok, tok)
+        rows = pl.ds(at, tok)
+        part = mm(nrm[rows, :depth], up_b[0])
+        for k in range(1, n):
+            part = part + mm(nrm[rows, k * depth : (k + 1) * depth], up_b[k])
+        pre[pl.ds(pl.multiple_of(at + 8, 8), tok)] = part.astype(bf16).astype(f32)
+
+    def finish(d):
+        receive(("nc", d), block(behind[d], tc), sib)
+        receive(("ncx", d), block(behind[d], tcx), sib)
+        lift(behind[d])
+
+    last = None
+    for d in order:
+        receive(("nz", d), block(behind[d], t), {"sp": ahead[d]})
+        send(("nx", d), block(behind[d], t), block(behind[d], t), side)
+        send(("nc", d), block(behind[d], t), block(behind[d], t), sib)
+    finish(0)
+    for d in order:
+        receive(("nx", d), block(behind[d], tx), side)
+        send(("ncx", d), block(behind[d], tx), block(behind[d], tx), sib)
+        if last is not None:
+            finish(last)
+        last = d
+    finish(last)
+
+    count = taps.shape[0]
+    for i in range(n):
+        conv = jnp.zeros((tok, pre.shape[1]), f32)
+        for k in range(count):
+            conv = conv + taps[k : k + 1] * pre[i * tok + 9 - count + k : i * tok + 9 - count + k + tok]
+        first = conv[:, :LANES]
+        last_block = conv[:, 2 * LANES :]
+        gated[i * tok : (i + 1) * tok, :LANES] = (
+            first / (1.0 + jnp.exp(-first)) * conv[:, LANES : 2 * LANES]
+        ).astype(bf16)
+        tail = last_block / (1.0 + jnp.exp(-last_block)) * pltpu.roll(last_block, HEAD, 1)
+        gated[i * tok : (i + 1) * tok, LANES:] = jnp.where(lane < HEAD, tail, 0.0).astype(bf16)
+
+    for d in ranks:
+        rows = pl.ds(pl.multiple_of(dhalf - dhalf * g, dhalf), dhalf)
+        receive(("dy", d), down_b.at[behind[d], rows], across)
+
+    def fold_core(d):
+        receive(("rc", d), c_r.at[d], sib)
+        x_s[d] = (keep[d, 1] + c_r[d, 1].astype(f32)).astype(bf16)
+        send(("rx", d), x_s.at[d], x_r.at[d], side)
+
+    previous = None
+    for d in order + [0]:
+        rows = pl.ds(pl.multiple_of(ahead[d] * tok, tok), tok)
+        piece = gated[rows]
+        for k in range(n):
+            proj[:, k * depth : (k + 1) * depth] = mm(piece, down_b[k])
+        keep[d, 0] = proj[chunk(t)]
+        keep[d, 1] = proj[chunk(tx)]
+        c_s[d, 0] = proj[chunk(tc)].astype(bf16)
+        c_s[d, 1] = proj[chunk(tcx)].astype(bf16)
+        send(("rc", d), c_s.at[d], c_r.at[d], sib)
+        if previous is not None:
+            fold_core(previous)
+        previous = d
+    fold_core(0)
+    for d in order:
+        receive(("rx", d), x_r.at[d], side)
+        z_s[d - 1] = (
+            keep[d, 0] + c_r[d, 0].astype(f32) + x_r[d].astype(f32)
+        ).astype(bf16)
+        send(("rz", d), z_s.at[d - 1], z_r.at[d - 1], {"sp": ahead[d]})
+    receive(("rx", 0), x_r.at[0], side)
+    result = state[...].astype(f32) + keep[0, 0] + c_r[0, 0].astype(f32) + x_r[0].astype(f32)
+    for d in order:
+        receive(("rz", d), z_r.at[d - 1], {"sp": ahead[d]})
+        result = result + z_r[d - 1].astype(f32)
+    out[...] = result.astype(bf16)
+    for copy in started:
+        copy.wait_send()
+
+
+def fast_body(
+    queries,
+    keys,
+    values,
+    resid,
+    out_weight,
+    gate_weight,
+    value_weight,
+    conv_gate,
+    conv_value,
+    norm_gain,
+    down_weight,
+):
+    n = lax.axis_size("sp")
+    tok = queries.shape[0]
+    share, width = resid.shape
+    depth, ff_local = gate_weight.shape
+    unit = ff_local // n
+
+    def by_rank(a):
+        return jnp.transpose(a.reshape(a.shape[0], n, -1), (1, 0, 2))
+
+    q, k, v = by_rank(queries), by_rank(keys), by_rank(values)
+    qkv = jnp.concatenate([q, jnp.zeros_like(q), k, v], axis=2)
+
+    def interleave(gate, value):
+        return jnp.concatenate(
+            [gate[..., :LANES], value[..., :LANES], gate[..., LANES:], value[..., LANES:]], axis=-1
+        )
+
+    up = interleave(by_rank(gate_weight), by_rank(value_weight))
+    mine = lax.axis_index("sp") * unit
+    taps = interleave(
+        lax.dynamic_slice_in_dim(conv_gate, mine, unit, 1),
+        lax.dynamic_slice_in_dim(conv_value, mine, unit, 1),
+    )
+    down = down_weight.reshape(n, unit, down_weight.shape[1])
+    vm = pl.BlockSpec(memory_space=pltpu.VMEM)
+    full = n * tok
+    return pl.pallas_call(
+        functools.partial(layer_kernel, n),
+        out_shape=jax.ShapeDtypeStruct((share, width), bf16),
+        in_specs=[vm] * 7,
+        out_specs=vm,
+        scratch_shapes=[
+            pltpu.VMEM(qkv.shape, bf16),
+            pltpu.VMEM(up.shape, bf16),
+            pltpu.VMEM((n, 2 * LANES, down.shape[2]), bf16),
+            pltpu.VMEM((n, tok, LANES), bf16),
+            pltpu.VMEM((n, tok, LANES), bf16),
+            pltpu.VMEM((tok, width), f32),
+            pltpu.VMEM((3, share, width), bf16),
+            pltpu.VMEM((3, share, width), bf16),
+            pltpu.VMEM((full, width), bf16),
+            pltpu.VMEM((full + 8, 2 * unit), f32),
+            pltpu.VMEM((full, 2 * LANES), bf16),
+            pltpu.VMEM((n, 2, share, width), f32),
+            pltpu.VMEM((n, 2, share, width), bf16),
+            pltpu.VMEM((n, 2, share, width), bf16),
+            pltpu.VMEM((n, share, width), bf16),
+            pltpu.VMEM((n, share, width), bf16),
+            pltpu.VMEM((n - 1, share, width), bf16),
+            pltpu.VMEM((n - 1, share, width), bf16),
+            pltpu.VMEM((share, width), bf16),
+            pltpu.SemaphoreType.DMA((64,)),
+            pltpu.SemaphoreType.DMA((64,)),
+        ],
+        compiler_params=pltpu.CompilerParams(
+            collective_id=0, has_side_effects=True, vmem_limit_bytes=60 * 1024 * 1024
+        ),
+    )(qkv, up, down, out_weight, resid, norm_gain.reshape(1, -1), taps)
+
+
+def fits(mesh, queries, gate_weight):
+    sizes = dict(mesh.shape)
+    n = sizes["sp"]
+    mix_local = queries.shape[1] // sizes["tp"]
+    unit = gate_weight.shape[1] // (sizes["tp"] * n)
+    return (
+        sizes["grp"] == 2
+        and sizes["tp"] == 4
+        and n % 2 == 0
+        and mix_local == n * HEAD
+        and unit == LANES + HEAD
+        and queries.shape[0] // (2 * n) == 256
+    )
+
+
 def solution(mesh):
     placed = (
         P(("grp", "sp"), "tp"),
@@ -135,6 +463,15 @@
         P(),
         P("tp", "sp"),
     )
-    return jax.shard_map(
-        body, mesh=mesh, in_specs=placed, out_specs=P(("grp", "sp", "tp"), None), check_vma=False
-    )
+
+    def run(*operands):
+        chosen = fast_body if fits(mesh, operands[0], operands[5]) else body
+        return jax.shard_map(
+            chosen,
+            mesh=mesh,
+            in_specs=placed,
+            out_specs=P(("grp", "sp", "tp"), None),
+            check_vma=False,
+        )(*operands)
+
+    return run

time: 384 us -> 142 us (0.37)
  waiting for transfers between devices: 292 us -> 0 us
  Pallas kernels: 0 us -> 130 us
  matrix products: 25.1 us -> 0 us
  other arithmetic: 25.9 us -> 3.23 us
  local copies, waits for them, and re-layouts: 25.4 us -> 7.71 us
  between operations: 13.7 us -> 0.16 us
    all_gather x5 -> x0, waiting for transfers between devices: 230 us -> none  [the longest x1 61.7 us: body(): lax.all_gather(gate_weight, 'sp', axis=0, tiled=True)]
    pallas_call x0 -> x1, Pallas kernels: none -> 130 us  [fast_body(): pl.pallas_call(functools.partial(layer_kernel, n), out_shape=jax.ShapeDty...]
    reduce_scatter x2 -> x0, waiting for transfers between devices: 58.8 us -> none  [the longest x1 30 us: body(): lax.psum_scatter(partial_sum, 'tp', scatter_dimension=0, tiled=True)]
    dot_general x6 -> x0, matrix products: 25.1 us -> none  [the longest x1 9.52 us: block_terms(): jnp.einsum('hqk,khe->hqe', local_weight, value_rows, preferred_element_ty...]
    another operation x3 -> x0, other arithmetic: 15.3 us -> none
    another operation x4 -> x0, local copies, waits for them, and re-layouts: 10.4 us -> none  [the longest x2 10.4 us: block_terms(): suffix = lax.cumsum(stay_log, axis=2, reverse=True) - stay_log]
    reduce_sum x2 -> x0, other arithmetic: 6.84 us -> none  [the longest x1 5.62 us: block_terms(): return (jnp.sum(stay_log, axis=2), part)]
    while x3 -> x0, local copies, waits for them, and re-layouts: 4.94 us -> none
  transfers between devices with their start and end apart: 8 -> 0, of which waited for: 8 -> 0; matrix products, arithmetic and copies ran while one was open for 2% -> 0% of each run, Pallas kernels for 0% -> 0%
where the time goes in v1:
time: 142 us
  Pallas kernels  130 us (92%)
  local copies, waits for them, and re-layouts  7.71 us (5%)
  other arithmetic  3.23 us (2%)
    pallas_call x1, Pallas kernels, fast_body(): pl.pallas_call(functools.partial(layer_kernel, n), out_shape=jax.ShapeDty...  130 us
    unnamed x14, local copies, waits for them, and re-layouts  4.18 us

profile of v1, /device:TPU:0, one launch (start us, length us, event | category | flops | bytes accessed | tf_op | source)
XLA Modules:
  0.0 141.5 jit_solution(10999274314804522660)
XLA Ops:
  0.0 0.8 constant_dynamic-slice_fusion.2
  0.8 0.8 constant_dynamic-slice_fusion
  1.5 0.7 pad_maximum_fusion.2.taps
  2.2 1.4 copy.18
  3.6 0.0 copy-start
  3.6 0.5 copy.19
  4.2 0.1 slice.32
  4.3 0.5 copy-done
  4.8 0.3 copy.20
  5.0 0.5 copy.21
  5.6 0.1 slice.33
  5.7 0.1 slice.34
  5.8 0.1 slice.35
  5.9 0.0 copy-start.1
  5.9 0.0 copy-start.2
  5.9 0.0 copy-start.3
  5.9 1.6 %pad_maximum_fusion.up = bf16[4,512,384]{2,1,0:T(8,128)(2,1)} fusion(bf16[4,512,64]{2,1,0:T(8,128)(2,1)S(1)} %slice.35, bf16[4,512,64]{2,1,0:T(8,128)(2,1)S(1)} %slice.34, bf16[4,512,128]{2,1,0:T(8,128)(2,1)S(1)} %slice.33, bf16[4,512,128]{2,1,0:T(8,128)(2,1)S(1)} %slice.32), kind=kLoop, calls=%fused_computation | loop fusion | flops 6291456 | bytes 3145728 | tf_op jit(solution)/shard_map/concatenate | solution.py:390
  7.5 0.0 copy-done.1
  7.5 0.1 copy.12
  7.6 0.2 copy.13
  7.7 0.0 copy-done.2
  7.8 0.1 copy.14
  7.9 0.2 copy.15
  8.0 0.0 copy-done.3
  8.1 0.1 copy.16
  8.2 0.2 copy.17
  8.3 0.1 pad.9.clone
  8.4 1.0 pad_maximum_fusion.1.qkv
  9.4 130.4 %shard_map.109 = bf16[64,2048]{1,0:T(8,128)(2,1)} custom-call(bf16[4,256,256]{2,1,0:T(8,128)(2,1)} %pad_maximum_fusion.1.qkv, bf16[4,512,384]{2,1,0:T(8,128)(2,1)} %pad_maximum_fusion.up, bf16[4,192,512]{2,1,0:T(8,128)(2,1)} %bitcast.21, bf16[256,2048]{1,0:T(8,128)(2,1)} %ow.1, bf16[64,2048]{1,0:T(8,128)(2,1)} %resid.1, f32[1,2048]{1,0:T(1,128)} %bitcast.25, ...), custom_call_target="tpu_custom_call" | custom-call | tf_op jit(solution)/shard_map/pallas_call | solution.py:403
  139.8 1.7 %copy.23 = bf16[64,2048]{1,0:T(8,128)(2,1)} copy(bf16[64,2048]{1,0:T(8,128)(2,1)} %shard_map.109) | data formatting | bytes 524288
  (1 shorter events, 0.0 us)
Async XLA Ops:
  3.6 1.1 copy-start
  5.9 1.6 %copy-start.1 = (bf16[256,256]{1,0:T(8,128)(2,1)S(1)}, bf16[256,256]{1,0:T(8,128)(2,1)}, u32[]{:S(2)}) copy-start(bf16[256,256]{1,0:T(8,128)(2,1)} %param.11) | copy-start | bytes 393220
  5.9 1.9 %copy-start.2 = (bf16[256,256]{1,0:T(8,128)(2,1)S(1)}, bf16[256,256]{1,0:T(8,128)(2,1)}, u32[]{:S(2)}) copy-start(bf16[256,256]{1,0:T(8,128)(2,1)} %param.12) | copy-start | bytes 393220
  5.9 2.2 %copy-start.3 = (bf16[256,256]{1,0:T(8,128)(2,1)S(1)}, bf16[256,256]{1,0:T(8,128)(2,1)}, u32[]{:S(2)}) copy-start(bf16[256,256]{1,0:T(8,128)(2,1)} %param.13) | copy-start | bytes 393220

commit v2 on v1

--- a/solution.py
+++ b/solution.py
@@ -182,9 +182,12 @@
 
     for d in ranks:
         send(("q", d), qkv.at[ahead[d]], qkv_b.at[s], {"sp": ahead[d]})
-    for d in ranks:
+
+    def send_up(d):
         rows = pl.ds(pl.multiple_of(half * g, half), half)
         send(("u", d), up.at[ahead[d], rows], up_b.at[s, rows], {"sp": ahead[d]})
+
+    send_up(1)
     qkv_b[s] = qkv[s]
     up_b[s] = up[s]
     down_b[:, 2 * dhalf :] = jnp.zeros((n, down_b.shape[1] - 2 * dhalf, down_b.shape[2]), bf16)
@@ -224,9 +227,8 @@
 
     for d in ranks:
         send(("m", d), mix_s.at[ahead[d]], mix_r.at[s], {"sp": ahead[d]})
-    for d in ranks:
-        rows = pl.ds(pl.multiple_of(dhalf * g, dhalf), dhalf)
-        send(("d", d), down.at[ahead[d], rows], down_b.at[s, rows], {"sp": ahead[d]})
+    for d in ranks[1:]:
+        send_up(d)
     mix_r[s] = mix_s[s]
     for d in ranks:
         receive(("m", d), mix_r.at[behind[d]], {"sp": ahead[d]})
@@ -248,10 +250,6 @@
         op_s[e - 1] = proj[chunk(to)].astype(bf16)
         send(("o", e), op_s.at[e - 1], op_r.at[e - 1], {"tp": to})
     across = {"grp": 1 - g}
-    for d in ranks:
-        rows = pl.ds(pl.multiple_of(half * g, half), half)
-        receive(("u", d), up_b.at[behind[d], rows], {"sp": ahead[d]})
-        send(("uy", d), up_b.at[behind[d], rows], up_b.at[behind[d], rows], across)
     for e in (1, 2, 3):
         receive(("o", e), op_r.at[e - 1], {"tp": lax.rem(t + e, 4)})
     summed = proj[chunk(t)] + op_r[0].astype(f32) + op_r[1].astype(f32) + op_r[2].astype(f32)
@@ -273,13 +271,13 @@
     send(("nc", 0), block(s, t), block(s, t), sib)
     for d in ranks:
         rows = pl.ds(pl.multiple_of(dhalf * g, dhalf), dhalf)
-        receive(("d", d), down_b.at[behind[d], rows], {"sp": ahead[d]})
-        send(("dy", d), down_b.at[behind[d], rows], down_b.at[behind[d], rows], across)
+        send(("d", d), down.at[ahead[d], rows], down_b.at[s, rows], {"sp": ahead[d]})
+    for d in ranks:
+        rows = pl.ds(pl.multiple_of(half * g, half), half)
+        receive(("u", d), up_b.at[behind[d], rows], {"sp": ahead[d]})
+        send(("uy", d), up_b.at[behind[d], rows], up_b.at[behind[d], rows], across)
     receive(("nx", 0), block(s, tx), side)
     send(("ncx", 0), block(s, tx), block(s, tx), sib)
-    for d in ranks:
-        rows = pl.ds(pl.multiple_of(half - half * g, half), half)
-        receive(("uy", d), up_b.at[behind[d], rows], across)
 
     def lift(si):
         at = pl.multiple_of(si * tok, tok)
@@ -299,6 +297,9 @@
         receive(("nz", d), block(behind[d], t), {"sp": ahead[d]})
         send(("nx", d), block(behind[d], t), block(behind[d], t), side)
         send(("nc", d), block(behind[d], t), block(behind[d], t), sib)
+    for d in ranks:
+        rows = pl.ds(pl.multiple_of(half - half * g, half), half)
+        receive(("uy", d), up_b.at[behind[d], rows], across)
     finish(0)
     for d in order:
         receive(("nx", d), block(behind[d], tx), side)
@@ -306,6 +307,10 @@
         if last is not None:
             finish(last)
         last = d
+    for d in ranks:
+        rows = pl.ds(pl.multiple_of(dhalf * g, dhalf), dhalf)
+        receive(("d", d), down_b.at[behind[d], rows], {"sp": ahead[d]})
+        send(("dy", d), down_b.at[behind[d], rows], down_b.at[behind[d], rows], across)
     finish(last)
 
     count = taps.shape[0]

time: 142 us -> 140 us (0.986)
  Pallas kernels: 130 us -> 128 us
    pallas_call x1, Pallas kernels: 130 us -> 128 us  [fast_body(): pl.pallas_call(functools.partial(layer_kernel, n), out_shape=jax.ShapeDty...]
where the time goes in v2:
time: 140 us; the launch traced here: 139 us
  Pallas kernels  128 us (91%)
  local copies, waits for them, and re-layouts  7.71 us (6%)
  other arithmetic  3.23 us (2%)
    pallas_call x1, Pallas kernels, fast_body(): pl.pallas_call(functools.partial(layer_kernel, n), out_shape=jax.ShapeDty...  128 us
    unnamed x14, local copies, waits for them, and re-layouts  4.18 us

profile of v2, /device:TPU:0, one launch (start us, length us, event | category | flops | bytes accessed | tf_op | source)
XLA Modules:
  0.0 139.2 jit_solution(3858180485695893660)
XLA Ops:
  0.0 0.8 constant_dynamic-slice_fusion.2
  0.8 0.8 constant_dynamic-slice_fusion
  1.5 0.7 pad_maximum_fusion.2.taps
  2.2 1.4 %copy.18 = bf16[512,768]{0,1:T(8,128)(2,1)S(1)} copy(bf16[512,768]{1,0:T(8,128)(2,1)} %param.16) | data formatting | bytes 1572864 | tf_op args[5]
  3.6 0.0 copy-start
  3.6 0.5 copy.19
  4.2 0.1 slice.32
  4.3 0.5 copy-done
  4.8 0.3 copy.20
  5.0 0.5 copy.21
  5.6 0.1 slice.33
  5.7 0.1 slice.34
  5.8 0.1 slice.35
  5.9 0.0 copy-start.1
  5.9 0.0 copy-start.2
  5.9 0.0 copy-start.3
  5.9 1.6 %pad_maximum_fusion.up = bf16[4,512,384]{2,1,0:T(8,128)(2,1)} fusion(bf16[4,512,64]{2,1,0:T(8,128)(2,1)S(1)} %slice.35, bf16[4,512,64]{2,1,0:T(8,128)(2,1)S(1)} %slice.34, bf16[4,512,128]{2,1,0:T(8,128)(2,1)S(1)} %slice.33, bf16[4,512,128]{2,1,0:T(8,128)(2,1)S(1)} %slice.32), kind=kLoop, calls=%fused_computation | loop fusion | flops 6291456 | bytes 3145728 | tf_op jit(solution)/shard_map/concatenate | solution.py:395
  7.5 0.0 copy-done.1
  7.5 0.1 copy.12
  7.6 0.2 copy.13
  7.7 0.0 copy-done.2
  7.8 0.1 copy.14
  7.9 0.2 copy.15
  8.0 0.0 copy-done.3
  8.1 0.1 copy.16
  8.2 0.2 copy.17
  8.3 0.1 pad.9.clone
  8.4 1.0 pad_maximum_fusion.1.qkv
  9.4 128.1 %shard_map.109 = bf16[64,2048]{1,0:T(8,128)(2,1)} custom-call(bf16[4,256,256]{2,1,0:T(8,128)(2,1)} %pad_maximum_fusion.1.qkv, bf16[4,512,384]{2,1,0:T(8,128)(2,1)} %pad_maximum_fusion.up, bf16[4,192,512]{2,1,0:T(8,128)(2,1)} %bitcast.21, bf16[256,2048]{1,0:T(8,128)(2,1)} %ow.1, bf16[64,2048]{1,0:T(8,128)(2,1)} %resid.1, f32[1,2048]{1,0:T(1,128)} %bitcast.25, ...), custom_call_target="tpu_custom_call" | custom-call | tf_op jit(solution)/shard_map/pallas_call | solution.py:408
  137.6 1.7 %copy.23 = bf16[64,2048]{1,0:T(8,128)(2,1)} copy(bf16[64,2048]{1,0:T(8,128)(2,1)} %shard_map.109) | data formatting | bytes 524288
  (1 shorter events, 0.0 us)
Async XLA Ops:
  3.6 1.1 copy-start
  5.9 1.6 %copy-start.1 = (bf16[256,256]{1,0:T(8,128)(2,1)S(1)}, bf16[256,256]{1,0:T(8,128)(2,1)}, u32[]{:S(2)}) copy-start(bf16[256,256]{1,0:T(8,128)(2,1)} %param.11) | copy-start | bytes 393220
  5.9 1.9 %copy-start.2 = (bf16[256,256]{1,0:T(8,128)(2,1)S(1)}, bf16[256,256]{1,0:T(8,128)(2,1)}, u32[]{:S(2)}) copy-start(bf16[256,256]{1,0:T(8,128)(2,1)} %param.12) | copy-start | bytes 393220
  5.9 2.2 %copy-start.3 = (bf16[256,256]{1,0:T(8,128)(2,1)S(1)}, bf16[256,256]{1,0:T(8,128)(2,1)}, u32[]{:S(2)}) copy-start(bf16[256,256]{1,0:T(8,128)(2,1)} %param.13) | copy-start | bytes 393220
